TPU v7x, 32 devices: a whole 2x2x4 slice. The times are simulated.
32 devices in a mesh: rep: 2 (over x), fs: 8 (over z, y), tp: 2 (over core).
Axes of the slice: x: 2, y: 2, z: 4, core: 2. Of those that a mesh axis runs over, the one named last changes fastest.
Arguments:
- tokens: bfloat16 [8192, 2048], P(('rep', 'fs'), 'tp'), may hold values from -6 to 6
- mix_gain: float32 [2048], replicated, may hold values from 0.1 to 1.9
- query_w: bfloat16 [2048, 2048], P('fs', 'tp'), may hold values from -0.125 to 0.125
- key_w: bfloat16 [2048, 2048], P('fs', 'tp'), may hold values from -0.125 to 0.125
- value_w: bfloat16 [2048, 4096], P('fs', 'tp'), may hold values from -0.125 to 0.125
- head_gain: float32 [8, 512], replicated, may hold values from 0.1 to 1.9
- out_w: bfloat16 [4096, 2048], P('tp', 'fs'), may hold values from -0.09375 to 0.09375
- chan_gain: float32 [2048], replicated, may hold values from 0.1 to 1.9
- up_w: bfloat16 [2048, 4096], P('fs', 'tp'), may hold values from -0.125 to 0.125
- down_w: bfloat16 [4096, 2048], P('tp', 'fs'), may hold values from -0.09375 to 0.09375
Outputs:
- layer_out: bfloat16 [8192, 2048], P(('rep', 'fs'), 'tp')
All inputs are finite; a program needn't handle non-finite values.
Results may differ from a plain program's by a relative error of at most 0.019.
Values may be sent and summed in bfloat16 or wider, within the bound.
A program may use at most 128 MiB of HBM per device.

v0:
```python
import jax
import jax.numpy as jnp
from jax import lax
from jax.sharding import PartitionSpec as P

DK = 256
DV = 512
BLOCK = 128


EPS = 1e-06
HEAD_EPS = 0.05
THETA = 10000.0


def norm_rows(rows, gain):
    values = rows.astype(jnp.float32)
    scale = lax.rsqrt(jnp.mean(values * values, axis=-1, keepdims=True) + EPS)
    return (values * scale * gain).astype(jnp.bfloat16)


def rotate(field, places):
    half = field.shape[-1] // 2
    inverse = THETA ** (-jnp.arange(half, dtype=jnp.float32) / half)
    angles = places[:, None] * inverse
    cosine = jnp.cos(angles)[:, None, :]
    sine = jnp.sin(angles)[:, None, :]
    first = field[..., :half]
    second = field[..., half:]
    return jnp.concatenate(
        [first * cosine - second * sine, second * cosine + first * sine], axis=-1
    )


def retain(query, keys, values, log_rate):
    count = query.shape[0] // BLOCK
    q_blocks = query.reshape(count, BLOCK, query.shape[1])
    k_blocks = keys.reshape(count, BLOCK, keys.shape[1])
    v_blocks = values.reshape(count, BLOCK, values.shape[1])
    place = jnp.arange(BLOCK, dtype=jnp.float32)
    offset = place[:, None] - place[None, :]
    mask = jnp.where(offset >= 0, jnp.exp(log_rate * jnp.maximum(offset, 0.0)), 0.0)
    q_decay = jnp.exp(log_rate * (place + 1.0))
    k_decay = jnp.exp(log_rate * (BLOCK - 1.0 - place))
    block_decay = jnp.exp(log_rate * BLOCK)

    def advance(state, item):
        q_part, k_part, v_part = item
        scores = jnp.dot(q_part, k_part.T, preferred_element_type=jnp.float32)
        weights = (scores * mask).astype(jnp.bfloat16)
        result = jnp.dot(weights, v_part, preferred_element_type=jnp.float32)
        q_scaled = (q_part.astype(jnp.float32) * q_decay[:, None]).astype(jnp.bfloat16)
        result = result + jnp.dot(
            q_scaled, state.astype(jnp.bfloat16), preferred_element_type=jnp.float32
        )
        k_scaled = (k_part.astype(jnp.float32) * k_decay[:, None]).astype(jnp.bfloat16)
        state = state * block_decay + jnp.dot(
            k_scaled.T, v_part, preferred_element_type=jnp.float32
        )
        return (state, result)

    start = jnp.zeros((query.shape[1], values.shape[1]), jnp.float32)
    _, outputs = lax.scan(advance, start, (q_blocks, k_blocks, v_blocks))
    return outputs.reshape(count * BLOCK, values.shape[1])


def shards(tokens, mix_gain, query_w, key_w, value_w, head_gain, out_w, chan_gain, up_w, down_w):
    rows = tokens.shape[0]
    local = query_w.shape[1] // DK
    whole = lax.all_gather(tokens, "tp", axis=1, tiled=True)
    normed = norm_rows(whole, mix_gain)
    pieces = (
        lax.all_gather(query_w, "fs", axis=0, tiled=True),
        lax.all_gather(key_w, "fs", axis=0, tiled=True),
        lax.all_gather(value_w, "fs", axis=0, tiled=True),
    )
    inputs = normed
    qraw, kraw, vraw = tuple(
        (jnp.dot(inputs, piece, preferred_element_type=jnp.float32) for piece in pieces)
    )
    places = jnp.arange(rows, dtype=jnp.int32).astype(jnp.float32)
    query = rotate(qraw.reshape(rows, local, DK), places).astype(jnp.bfloat16)
    keys = (rotate(kraw.reshape(rows, local, DK), places) * DK ** (-0.5)).astype(jnp.bfloat16)
    values = vraw.reshape(rows, local, DV).astype(jnp.bfloat16)
    first_head = lax.axis_index("tp") * local
    heads = (first_head + jnp.arange(local, dtype=jnp.int32)).astype(jnp.float32)
    log_rate = jnp.log1p(-jnp.exp2(-5.0 - heads))
    retained = jax.vmap(retain, in_axes=(1, 1, 1, 0), out_axes=1)(query, keys, values, log_rate)
    gains = lax.dynamic_slice_in_dim(head_gain, first_head, local, 0)
    scale = lax.rsqrt(jnp.mean(retained * retained, axis=-1, keepdims=True) + HEAD_EPS)
    head_out = (retained * scale * gains).astype(jnp.bfloat16).reshape(rows, local * DV)
    mixer_terms = jnp.dot(
        head_out,
        lax.all_gather(out_w, "fs", axis=1, tiled=True),
        preferred_element_type=jnp.float32,
    )
    mixed = lax.psum_scatter(
        mixer_terms.astype(jnp.bfloat16), "tp", scatter_dimension=1, tiled=True
    ).astype(jnp.float32)
    middle = (tokens.astype(jnp.float32) + mixed).astype(jnp.bfloat16)
    whole_middle = lax.all_gather(middle, "tp", axis=1, tiled=True)
    chan_normed = norm_rows(whole_middle, chan_gain)
    inputs = chan_normed
    upward = jnp.dot(
        inputs, lax.all_gather(up_w, "fs", axis=0, tiled=True), preferred_element_type=jnp.float32
    )
    hidden = jnp.square(jax.nn.relu(upward)).astype(jnp.bfloat16)
    chan_terms = jnp.dot(
        hidden, lax.all_gather(down_w, "fs", axis=1, tiled=True), preferred_element_type=jnp.float32
    )
    channel = lax.psum_scatter(
        chan_terms.astype(jnp.bfloat16), "tp", scatter_dimension=1, tiled=True
    ).astype(jnp.float32)
    return (middle.astype(jnp.float32) + channel).astype(jnp.bfloat16)


def solution(mesh):
    placed = (
        P(("rep", "fs"), "tp"),
        P(),
        P("fs", "tp"),
        P("fs", "tp"),
        P("fs", "tp"),
        P(),
        P("tp", "fs"),
        P(),
        P("fs", "tp"),
        P("tp", "fs"),
    )
    return jax.shard_map(
        shards, mesh=mesh, in_specs=placed, out_specs=P(("rep", "fs"), "tp"), check_vma=False
    )
```

profile of v0, /device:TPU:0, one launch (start us, length us, event | category | flops | bytes accessed | tf_op | source)
XLA Modules:
  0.0 740.9 jit_solution(1086600032744089583)
XLA Ops:
  6.5 0.7 all-gather.9.cloned.1.call-update
  7.3 0.7 all-gather.11.cloned.1.call-update
  8.1 0.7 all-gather.15.cloned.1.call-update
  8.8 0.5 all-gather.13.cloned.1.call-update
  9.4 0.5 all-gather.17.cloned.1.call-update
  10.1 1.8 multiply_cosine_fusion
  11.9 10.3 %all-gather.9.cloned.1.call-done = bf16[512,2048]{1,0:T(8,128)(2,1)} async-done(((bf16[512,1024]{1,0:T(8,128)(2,1)}), bf16[512,2048]{1,0:T(8,128)(2,1)}) %all-gather.9.cloned.1.call-update) | async-done | bytes 2097168 | tf_op jit(solution)/shard_map/all_gather | solution.py:70
  22.2 2.1 fusion.42
  24.3 74.0 %all-gather.11.cloned.1.call-done = bf16[2048,1024]{1,0:T(8,128)(2,1)} async-done(((bf16[256,1024]{1,0:T(8,128)(2,1)}), bf16[2048,1024]{1,0:T(8,128)(2,1)}) %all-gather.11.cloned.1.call-update) | async-done | bytes 4194320 | tf_op jit(solution)/shard_map/all_gather | solution.py:74
  98.3 6.5 fusion.60
  104.8 3.2 reshape.151
  108.1 63.8 %all-gather.15.cloned.1.call-done = bf16[2048,1024]{1,0:T(8,128)(2,1)} async-done(((bf16[256,1024]{1,0:T(8,128)(2,1)}), bf16[2048,1024]{1,0:T(8,128)(2,1)}) %all-gather.15.cloned.1.call-update) | async-done | bytes 4194320 | tf_op jit(solution)/shard_map/all_gather | solution.py:73
  171.8 6.6 fusion.57
  178.4 3.3 reshape.154
  181.7 2.8 fusion.62
  184.4 0.6 subtract_convert_fusion
  185.0 1.1 pad_maximum_fusion
  186.1 1.1 fusion.52
  187.3 109.6 %all-gather.13.cloned.1.call-done = bf16[2048,2048]{1,0:T(8,128)(2,1)} async-done(((bf16[256,2048]{1,0:T(8,128)(2,1)}), bf16[2048,2048]{1,0:T(8,128)(2,1)}) %all-gather.13.cloned.1.call-update) | async-done | bytes 8388624 | tf_op jit(solution)/shard_map/all_gather | solution.py:75
  296.8 8.6 %convolution_convert_fusion.2 = bf16[512,2048]{1,0:T(8,128)(2,1)S(1)} fusion(bf16[2048,2048]{1,0:T(8,128)(2,1)} %all-gather.13.cloned.1.call-done, bf16[512,2048]{1,0:T(8,128)(2,1)} %all-gather.9.cloned.1.call-done, f32[2048]{0:T(1024)S(1)} %copy-done.7, f32[512]{0:T(512)S(1)} %add_rsqrt_fusion.2), kind=kOutput, calls=%fused_computation.62 | convolution fusion | flops 4300210176 | bytes 12593152 | tf_op jit(solution)/shard_map/dot_general | solution.py:79
  305.4 1.5 copy.43
  306.9 27.4 %while.15 = (s32[]{:T(128)}, f32[4,256,512]{2,1,0:T(8,128)S(1)}, f32[4,4,128,512]{3,2,0,1:T(8,128)}, bf16[4,4,128,256]{3,2,0,1:T(8,128)(2,1)}, bf16[4,4,128,512]...) while((s32[]{:T(128)}, f32[4,256,512]{2,1,0:T(8,128)S(1)}, ...), condition=%wide.region_2.3_spmd.clone.clone.clone, body=%wide.region_1.2_spmd.clone.clone.clone.sunk | while | flops 372507680 | bytes 12677336 | solution.py:63
  306.9 0.1 multiply_exponential_fusion.6
  307.0 1.3 fusion.90
  308.3 2.7 fusion.91
  311.0 1.0 constant_dynamic-slice_fusion.5
  312.0 0.2 copy.45
  312.2 1.6 multiply_add_fusion.3
  313.8 0.1 multiply_exponential_fusion.6
  313.9 1.3 fusion.90
  315.2 2.6 fusion.91
  317.8 1.0 constant_dynamic-slice_fusion.5
  318.8 0.2 copy.45
  319.0 1.6 multiply_add_fusion.3
  320.6 0.1 multiply_exponential_fusion.6
  320.7 1.3 fusion.90
  322.0 2.7 fusion.91
  324.7 1.0 constant_dynamic-slice_fusion.5
  325.7 0.2 copy.45
  325.9 1.6 multiply_add_fusion.3
  327.5 0.1 multiply_exponential_fusion.6
  327.6 1.3 fusion.90
  328.9 2.7 fusion.91
  331.6 1.0 constant_dynamic-slice_fusion.5
  332.6 0.2 copy.45
  332.7 1.6 multiply_add_fusion.3
  334.4 2.7 fusion.48
  337.1 0.8 copy-done.2
  337.9 0.5 fusion.50
  338.3 2.6 copy.20
  340.9 80.9 %all-gather.17.cloned.1.call-done = bf16[2048,2048]{1,0:T(8,128)(2,1)} async-done(((bf16[2048,256]{1,0:T(8,128)(2,1)}), bf16[2048,2048]{1,0:T(8,128)(2,1)}) %all-gather.17.cloned.1.call-update) | async-done | bytes 8388624 | tf_op jit(solution)/shard_map/all_gather | solution.py:94
  421.9 10.0 %convolution_convert_fusion.1 = bf16[512,2048]{1,0:T(8,128)(2,1)} fusion(bf16[512,2048]{0,1:T(8,128)(2,1)} %bitcast.94, bf16[2048,2048]{1,0:T(8,128)(2,1)} %all-gather.17.cloned.1.call-done), kind=kOutput, calls=%fused_computation.61 | convolution fusion | flops 4296015872 | bytes 12582912 | tf_op jit(solution)/shard_map/dot_general | solution.py:92
  431.9 0.0 all-gather.19.cloned.1.call-start
  431.9 7.9 %reduce-scatter.3.cloned.1.call-done = bf16[512,1024]{1,0:T(8,128)(2,1)} async-done(((bf16[512,2048]{1,0:T(8,128)(2,1)}), bf16[512,1024]{1,0:T(8,128)(2,1)}) %reduce-scatter.3.cloned.1.call-update) | async-done | bytes 1048592 | tf_op jit(solution)/shard_map/reduce_scatter | solution.py:97
  439.8 2.6 add_convert_fusion.1
  442.5 0.7 all-gather.21.cloned.1.call-update
  443.3 0.7 all-gather.23.cloned.1.call-update
  444.0 10.5 %all-gather.19.cloned.1.call-done = bf16[512,2048]{1,0:T(8,128)(2,1)} async-done(((bf16[512,1024]{1,0:T(8,128)(2,1)}), bf16[512,2048]{1,0:T(8,128)(2,1)}) %all-gather.19.cloned.1.call-update) | async-done | bytes 2097168 | tf_op jit(solution)/shard_map/all_gather | solution.py:101
  454.5 2.2 fusion.45
  456.7 125.6 %all-gather.21.cloned.1.call-done = bf16[2048,2048]{1,0:T(8,128)(2,1)} async-done(((bf16[256,2048]{1,0:T(8,128)(2,1)}), bf16[2048,2048]{1,0:T(8,128)(2,1)}) %all-gather.21.cloned.1.call-update) | async-done | bytes 8388624 | tf_op jit(solution)/shard_map/all_gather | solution.py:105
  582.3 125.2 %all-gather.23.cloned.1.call-done = bf16[2048,2048]{1,0:T(8,128)(2,1)} async-done(((bf16[2048,256]{1,0:T(8,128)(2,1)}), bf16[2048,2048]{1,0:T(8,128)(2,1)}) %all-gather.23.cloned.1.call-update) | async-done | bytes 8388624 | tf_op jit(solution)/shard_map/all_gather | solution.py:109
  707.5 16.0 %convolution_convert_fusion = bf16[512,2048]{1,0:T(8,128)(2,1)} fusion(bf16[2048,2048]{1,0:T(8,128)(2,1)} %all-gather.23.cloned.1.call-done, bf16[2048,2048]{1,0:T(8,128)(2,1)} %all-gather.21.cloned.1.call-done, bf16[512,2048]{1,0:T(8,128)(2,1)S(1)} %copy-done.5, f32[2048]{0:T(1024)S(1)} %copy-done.8, f32[512]{0:T(512)S(1)} %add_rsqrt_fusion.1), kind=kOutput, calls=%fused_computation.60 | convolution fusion | flops 8598323200 | bytes 20981760 | tf_op jit(solution)/shard_map/dot_general | solution.py:108
  723.5 7.9 %reduce-scatter.5.cloned.1.call-done = bf16[512,1024]{1,0:T(8,128)(2,1)} async-done(((bf16[512,2048]{1,0:T(8,128)(2,1)}), bf16[512,1024]{1,0:T(8,128)(2,1)}) %reduce-scatter.5.cloned.1.call-update) | async-done | bytes 1048592 | tf_op jit(solution)/shard_map/reduce_scatter | solution.py:111
  731.4 2.6 add_convert_fusion
  (45 shorter events, 0.6 us)
Async XLA Ops:
  6.5 3.5 copy-start
  6.5 15.7 %all-gather.9.cloned.1.call-start = ((), (), s32[]{:S(2)}) async-start(), calls=%async_computation.2 | async-start | bytes 3145728 | tf_op jit(solution)/shard_map/all_gather | solution.py:70
  7.3 91.1 %all-gather.11.cloned.1.call-start = ((), (), s32[]{:S(2)}) async-start(), calls=%async_computation.3 | async-start | bytes 4718592 | tf_op jit(solution)/shard_map/all_gather | solution.py:74
  8.0 163.8 %all-gather.15.cloned.1.call-start = ((), (), s32[]{:S(2)}) async-start(), calls=%async_computation.5 | async-start | bytes 4718592 | tf_op jit(solution)/shard_map/all_gather | solution.py:73
  8.7 288.1 %all-gather.13.cloned.1.call-start = ((), (), s32[]{:S(2)}) async-start(), calls=%async_computation.4 | async-start | bytes 9437184 | tf_op jit(solution)/shard_map/all_gather | solution.py:75
  9.3 89.0 %copy-start.7 = (f32[2048]{0:T(1024)S(1)}, f32[2048]{0:T(1024)}, u32[]{:S(2)}) copy-start(f32[2048]{0:T(1024)} %param.13) | copy-start | bytes 24580
  9.3 412.6 %all-gather.17.cloned.1.call-start = ((), (), s32[]{:S(2)}) async-start(), calls=%async_computation.6 | async-start | bytes 9437184 | tf_op jit(solution)/shard_map/all_gather | solution.py:94
  9.9 429.9 %reduce-scatter.3.cloned.1.call-start = ((), (), s32[]{:S(2)}) async-start(), calls=%async_computation.7 | async-start | bytes 3145728 | tf_op jit(solution)/shard_map/reduce_scatter | solution.py:97
  181.7 2.8 copy-start.6
  334.4 3.5 copy-start.2
  431.8 8.0 %copy-start.4 = (bf16[512,1024]{1,0:T(8,128)(2,1)S(1)}, bf16[512,1024]{1,0:T(8,128)(2,1)}, u32[]{:S(2)}) copy-start(bf16[512,1024]{1,0:T(8,128)(2,1)} %param.12) | copy-start | bytes 3145732
  431.9 22.6 %all-gather.19.cloned.1.call-start = ((), (), s32[]{:S(2)}) async-start(), calls=%async_computation.8 | async-start | bytes 3145728 | tf_op jit(solution)/shard_map/all_gather | solution.py:101
  442.4 265.0 %copy-start.8 = (f32[2048]{0:T(1024)S(1)}, f32[2048]{0:T(1024)}, u32[]{:S(2)}) copy-start(f32[2048]{0:T(1024)} %param.19) | copy-start | bytes 24580
  442.5 139.8 %all-gather.21.cloned.1.call-start = ((), (), s32[]{:S(2)}) async-start(), calls=%async_computation.9 | async-start | bytes 9437184 | tf_op jit(solution)/shard_map/all_gather | solution.py:105
  443.2 264.3 %all-gather.23.cloned.1.call-start = ((), (), s32[]{:S(2)}) async-start(), calls=%async_computation.10 | async-start | bytes 9437184 | tf_op jit(solution)/shard_map/all_gather | solution.py:109
  443.9 287.5 %reduce-scatter.5.cloned.1.call-start = ((), (), s32[]{:S(2)}) async-start(), calls=%async_computation.11 | async-start | bytes 3145728 | tf_op jit(solution)/shard_map/reduce_scatter | solution.py:111
  454.5 253.0 %copy-start.5 = (bf16[512,2048]{1,0:T(8,128)(2,1)S(1)}, bf16[512,2048]{1,0:T(8,128)(2,1)}, u32[]{:S(2)}) copy-start(bf16[512,2048]{1,0:T(8,128)(2,1)} %all-gather.19.cloned.1.call-done) | copy-start | bytes 6291460
  723.5 8.0 %copy-start.3 = (bf16[512,1024]{1,0:T(8,128)(2,1)S(1)}, bf16[512,1024]{1,0:T(8,128)(2,1)}, u32[]{:S(2)}) copy-start(bf16[512,1024]{1,0:T(8,128)(2,1)} %add_convert_fusion.1) | copy-start | bytes 3145732
  723.5 10.5 %copy-start.1 = (f32[8,512]{1,0:T(8,128)S(1)}, f32[8,512]{1,0:T(8,128)}, u32[]{:S(2)}) copy-start(f32[8,512]{1,0:T(8,128)} %param.17) | copy-start | bytes 49156
Sparse Core Ops, SparseCore 0:
  8.9 13.2 all-gather.8
  24.3 73.9 all-gather.10
  100.5 71.3 all-gather.14
  173.8 122.9 all-gather.12
  298.7 123.1 all-gather.16
  432.0 7.7 reduce-scatter.2
  442.6 11.8 all-gather.18
  456.6 125.6 all-gather.20
  584.3 123.1 all-gather.22
  723.6 7.7 reduce-scatter.4
where the time goes:
time: 742 us; the launch traced here: 741 us
  waiting for transfers between devices  620 us (84%)
  matrix products  70 us (9%)
  local copies, waits for them, and re-layouts  18.8 us (3%)
  other arithmetic  17.7 us (2%)
  between operations  13.7 us (2%)
    all_gather x1, waiting for transfers between devices, shards(): lax.all_gather(up_w, 'fs', axis=0, tiled=True)  126 us
    all_gather x1, waiting for transfers between devices, shards(): lax.all_gather(down_w, 'fs', axis=1, tiled=True)  125 us
    all_gather x1, waiting for transfers between devices, shards(): lax.all_gather(value_w, 'fs', axis=0, tiled=True)  110 us
    all_gather x1, waiting for transfers between devices, shards(): lax.all_gather(out_w, 'fs', axis=1, tiled=True)  80.9 us
    all_gather x1, waiting for transfers between devices, shards(): lax.all_gather(key_w, 'fs', axis=0, tiled=True)  74 us
    all_gather x1, waiting for transfers between devices, shards(): lax.all_gather(query_w, 'fs', axis=0, tiled=True)  63.8 us
    dot_general x3, matrix products, shards(): jnp.dot(inputs, piece, preferred_element_type=jnp.float32)  21.6 us
    dot_general x1, matrix products, shards(): jnp.dot(hidden, lax.all_gather(down_w, 'fs', axis=1, tiled=True), preferr...  16 us
  transfers between devices with their start and end apart: 10, of which 10 were waited for; matrix products, arithmetic and copies ran while one was open for 10% of the time, Pallas kernels for 0%

commit v1 on v0

--- a/solution.py
+++ b/solution.py
@@ -114,6 +114,72 @@
     return (middle.astype(jnp.float32) + channel).astype(jnp.bfloat16)
 
 
+def half_of(block, axis, index, count):
+    size = block.shape[axis] // count
+    return lax.dynamic_slice_in_dim(block, index * size, size, axis)
+
+
+def split_shards(
+    parts, tps, tokens, mix_gain, query_w, key_w, value_w, head_gain, out_w, chan_gain, up_w, down_w
+):
+    rows, width = tokens.shape
+    group = ("rep", "tp")
+    rep = lax.axis_index("rep")
+
+    def join(block):
+        whole = lax.all_gather(block, group, axis=0, tiled=False)
+        whole = whole.reshape(parts, tps, rows, width).transpose(0, 2, 1, 3)
+        return whole.reshape(parts * rows, tps * width)
+
+    def scatter(terms):
+        pieces = terms.astype(jnp.bfloat16).reshape(parts, rows, tps, width).transpose(0, 2, 1, 3)
+        pieces = pieces.reshape(parts * tps * rows, width)
+        return lax.psum_scatter(pieces, group, scatter_dimension=0, tiled=True).astype(jnp.float32)
+
+    local = query_w.shape[1] // DK // parts
+    mine = jnp.concatenate(
+        [half_of(w, 1, rep, parts) for w in (query_w, key_w, value_w)], axis=1
+    )
+    normed = norm_rows(join(tokens), mix_gain)
+    raw = jnp.dot(
+        normed,
+        lax.all_gather(mine, "fs", axis=0, tiled=True),
+        preferred_element_type=jnp.float32,
+    )
+    qraw, kraw, vraw = jnp.split(raw, [local * DK, 2 * local * DK], axis=1)
+    places = jnp.arange(rows, dtype=jnp.int32).astype(jnp.float32)
+    places = jnp.tile(places, parts)
+    query = rotate(qraw.reshape(parts * rows, local, DK), places).astype(jnp.bfloat16)
+    keys = (rotate(kraw.reshape(parts * rows, local, DK), places) * DK ** (-0.5)).astype(
+        jnp.bfloat16
+    )
+    values = vraw.reshape(parts * rows, local, DV).astype(jnp.bfloat16)
+    first_head = (lax.axis_index("tp") * parts + rep) * local
+    heads = (first_head + jnp.arange(local, dtype=jnp.int32)).astype(jnp.float32)
+    log_rate = jnp.log1p(-jnp.exp2(-5.0 - heads))
+    over_heads = jax.vmap(retain, in_axes=(1, 1, 1, 0), out_axes=1)
+    over_sequences = jax.vmap(over_heads, in_axes=(0, 0, 0, None), out_axes=0)
+    retained = over_sequences(
+        query.reshape(parts, rows, local, DK),
+        keys.reshape(parts, rows, local, DK),
+        values.reshape(parts, rows, local, DV),
+        log_rate,
+    ).reshape(parts * rows, local, DV)
+    gains = lax.dynamic_slice_in_dim(head_gain, first_head, local, 0)
+    scale = lax.rsqrt(jnp.mean(retained * retained, axis=-1, keepdims=True) + HEAD_EPS)
+    head_out = (retained * scale * gains).astype(jnp.bfloat16).reshape(parts * rows, local * DV)
+    out_all = lax.all_gather(half_of(out_w, 0, rep, parts), "fs", axis=1, tiled=True)
+    mixed = scatter(jnp.dot(head_out, out_all, preferred_element_type=jnp.float32))
+    middle = (tokens.astype(jnp.float32) + mixed).astype(jnp.bfloat16)
+    chan_normed = norm_rows(join(middle), chan_gain)
+    up_all = lax.all_gather(half_of(up_w, 1, rep, parts), "fs", axis=0, tiled=True)
+    upward = jnp.dot(chan_normed, up_all, preferred_element_type=jnp.float32)
+    hidden = jnp.square(jax.nn.relu(upward)).astype(jnp.bfloat16)
+    down_all = lax.all_gather(half_of(down_w, 0, rep, parts), "fs", axis=1, tiled=True)
+    channel = scatter(jnp.dot(hidden, down_all, preferred_element_type=jnp.float32))
+    return (middle.astype(jnp.float32) + channel).astype(jnp.bfloat16)
+
+
 def solution(mesh):
     placed = (
         P(("rep", "fs"), "tp"),
@@ -127,6 +193,13 @@
         P("fs", "tp"),
         P("tp", "fs"),
     )
+    parts, tps = mesh.shape["rep"], mesh.shape["tp"]
+
+    def body(*blocks):
+        if blocks[2].shape[1] // DK % parts == 0:
+            return split_shards(parts, tps, *blocks)
+        return shards(*blocks)
+
     return jax.shard_map(
-        shards, mesh=mesh, in_specs=placed, out_specs=P(("rep", "fs"), "tp"), check_vma=False
-    )
+        body, mesh=mesh, in_specs=placed, out_specs=P(("rep", "fs"), "tp"), check_vma=False
+    )

time: 742 us -> 617 us (0.83); the launches traced: 741 us -> 608 us
  waiting for transfers between devices: 620 us -> 382 us
  local copies, waits for them, and re-layouts: 18.8 us -> 122 us
    all_gather x8 -> x6, waiting for transfers between devices: 600 us -> 295 us  [the longest x1 104 us: split_shards(): lax.all_gather(mine, 'fs', axis=0, tiled=True)]
    reduce_scatter x2, waiting for transfers between devices: 15.8 us -> 85.8 us  [scatter(): lax.psum_scatter(pieces, group, scatter_dimension=0, tiled=True)]
    unnamed x18 -> x52, local copies, waits for them, and re-layouts: 0.8 us -> 32.5 us
    convert_element_type x2 -> x4, local copies, waits for them, and re-layouts: 4.14 us -> 27.6 us  [the longest x2 19.5 us: norm_rows(): values = rows.astype(jnp.float32)]
    reshape x2 -> x4, local copies, waits for them, and re-layouts: 6.5 us -> 22.7 us  [the longest x2 15.6 us: scatter(): terms.astype(jnp.bfloat16).reshape(parts, rows, tps, width)]
    transpose x0 -> x3, local copies, waits for them, and re-layouts: none -> 14.4 us  [the longest x2 11.2 us: scatter(): terms.astype(jnp.bfloat16).reshape(parts, rows, tps, width)]
    dot_general x5 -> x3, matrix products: 47.6 us -> 40.9 us  [the longest x1 15.6 us: split_shards(): jnp.dot(hidden, down_all, preferred_element_type=jnp.float32)]
  transfers between devices with their start and end apart: 10 -> 8, of which waited for: 10 -> 7; matrix products, arithmetic and copies ran while one was open for 10% -> 25% of each run, Pallas kernels for 0% -> 0%
where the time goes in v1:
time: 617 us; the launch traced here: 608 us
  waiting for transfers between devices  382 us (62%)
  local copies, waits for them, and re-layouts  122 us (20%)
  matrix products  65.3 us (11%)
  other arithmetic  23.9 us (4%)
  between operations  14.2 us (2%)
    all_gather x1, waiting for transfers between devices, split_shards(): lax.all_gather(mine, 'fs', axis=0, tiled=True)  104 us
    reduce_scatter x2, waiting for transfers between devices, scatter(): lax.psum_scatter(pieces, group, scatter_dimension=0, tiled=True)  85.8 us
    all_gather x1, waiting for transfers between devices, split_shards(): lax.all_gather(half_of(down_w, 0, rep, parts), 'fs', axis=1, tiled=True)  75.2 us
    all_gather x2, waiting for transfers between devices, join(): whole = lax.all_gather(block, group, axis=0, tiled=False)  62.4 us
    all_gather x1, waiting for transfers between devices, split_shards(): lax.all_gather(half_of(up_w, 1, rep, parts), 'fs', axis=0, tiled=True)  53 us
    unnamed x52, local copies, waits for them, and re-layouts  32.5 us
    convert_element_type x2, local copies, waits for them, and re-layouts, norm_rows(): values = rows.astype(jnp.float32)  19.5 us
    dot_general x1, matrix products, split_shards(): jnp.dot(hidden, down_all, preferred_element_type=jnp.float32)  15.6 us
  transfers between devices with their start and end apart: 8, of which 7 were waited for; matrix products, arithmetic and copies ran while one was open for 25% of the time, Pallas kernels for 0%

profile of v1, /device:TPU:0, one launch (start us, length us, event | category | flops | bytes accessed | tf_op | source)
XLA Modules:
  0.0 607.8 jit_solution(10356832514366758110)
XLA Ops:
  7.8 1.1 constant_dynamic-slice_fusion.6
  8.9 1.1 pad_maximum_fusion
  10.0 0.9 constant_dynamic-slice_fusion.4
  13.1 3.1 multiply_cosine_fusion
  16.2 29.9 %all-gather.17.cloned.1.call-done = bf16[2048,1024]{1,0:T(8,128)(2,1)} async-done(((bf16[512,1024]{1,0:T(8,128)(2,1)}), bf16[2048,1024]{1,0:T(8,128)(2,1)}) %all-gather.17.cloned.1.call-update) | async-done | bytes 4194320 | tf_op jit(solution)/shard_map/all_gather | solution.py:130
  46.1 9.8 %copy.76 = f32[2,2,512,1024]{3,1,2,0:T(2,128)} copy(bf16[2,2,512,1024]{3,2,1,0:T(8,128)(2,1)} %bitcast.107) | data formatting | bytes 12582912 | tf_op jit(solution)/shard_map/convert_element_type | solution.py:17
  55.9 11.5 %copy.110 = f32[128,8,2,1024]{3,1,2,0:T(8,128)} copy(f32[128,8,2,1024]{3,2,1,0:T(2,128)} %bitcast.104) | data formatting | bytes 16777216
  67.4 0.9 multiply_reduce_fusion.1
  68.3 104.4 %all-gather.9.cloned.1.call-done = bf16[2048,2048]{1,0:T(8,128)(2,1)} async-done(((bf16[256,2048]{1,0:T(8,128)(2,1)}), bf16[2048,2048]{1,0:T(8,128)(2,1)}) %all-gather.9.cloned.1.call-update) | async-done | bytes 8388624 | tf_op jit(solution)/shard_map/all_gather | solution.py:146
  172.7 14.2 %fusion.24 = f32[1024,2048]{1,0:T(8,128)S(1)} fusion(bf16[2048,2048]{1,0:T(8,128)(2,1)} %all-gather.9.cloned.1.call-done, f32[1024,2048]{1,0:T(8,128)} %bitcast.117, f32[2048]{0:T(1024)S(1)} %copy-done.27, f32[1024]{0:T(1024)S(1)} %bitcast.130), kind=kOutput, calls=%fused_computation.38 | convolution fusion | flops 8596226048 | bytes 25178112 | tf_op jit(solution)/shard_map/dot_general | solution.py:144
  187.0 2.9 fusion.36
  189.8 1.7 copy-done.8
  191.5 3.5 reshape.232
  195.1 2.6 fusion.37
  197.7 3.6 reshape.229
  201.3 1.8 fusion.38
  203.4 2.0 subtract_convert_fusion
  205.5 3.9 split.17
  209.3 4.6 convert_element_type.142
  214.0 3.5 copy.80
  217.4 1.1 pad_maximum_fusion.1
  218.7 38.8 %while.15 = (s32[]{:T(128)}, f32[2,2,256,512]{3,2,1,0:T(8,128)S(1)}, f32[4,2,2,128,512]{4,3,0,2,1:T(8,128)}, bf16[4,2,2,128,256]{4,3,0,1,2:T(8,128)(2,1)S(1)}, b...) while((s32[]{:T(128)}, ...), condition=%wide.region_3.4_spmd.clone.clone.clone, body=%wide.region_2.3_spmd.clone.clone.clone.sunk | while | flops 372441600 | bytes 21330904 | solution.py:63
  218.8 1.9 constant_dynamic-slice_fusion.9
  221.3 1.3 fusion.49
  222.7 0.9 exponential_select_fusion.2
  223.6 2.6 fusion.50
  226.2 2.2 multiply_add_fusion.3
  228.5 1.9 constant_dynamic-slice_fusion.9
  231.0 1.3 fusion.49
  232.4 0.9 exponential_select_fusion.2
  233.3 2.6 fusion.50
  235.9 2.2 multiply_add_fusion.3
  238.2 1.9 constant_dynamic-slice_fusion.9
  240.7 1.3 fusion.49
  242.1 0.9 exponential_select_fusion.2
  243.0 2.5 fusion.50
  245.6 2.2 multiply_add_fusion.3
  247.9 1.9 constant_dynamic-slice_fusion.9
  250.4 1.3 fusion.49
  251.8 0.9 exponential_select_fusion.2
  252.7 2.6 fusion.50
  255.3 2.2 multiply_add_fusion.3
  257.5 2.5 multiply_reduce_fusion.2
  260.3 1.6 mul.349
  261.9 3.0 copy.114
  265.0 3.2 copy.88
  268.2 3.0 copy.113
  271.2 11.2 %convolution_convert_fusion.1 = bf16[1024,2048]{1,0:T(8,128)(2,1)} fusion(bf16[1024,2048]{1,0:T(8,128)(2,1)} %all-gather.11.cloned.1.call-done, f32[1024,1024]{1,0:T(8,128)} %bitcast.121, f32[1024,1024]{1,0:T(8,128)} %bitcast.120, f32[1024]{0:T(1024)S(1)} %bitcast.128), kind=kOutput, calls=%fused_computation.49 | convolution fusion | flops 4300210176 | bytes 16781312 | tf_op jit(solution)/shard_map/dot_general | solution.py:172
  282.4 7.8 %reshape.236 = bf16[2,512,2,1024]{3,2,1,0:T(2,128)(2,1)} reshape(bf16[1024,2048]{1,0:T(8,128)(2,1)} %convolution_convert_fusion.1) | data formatting | bytes 8388608 | tf_op jit(solution)/shard_map/reshape | solution.py:135
  290.2 5.5 copy.90
  295.8 42.9 %reduce-scatter.3.cloned.1.call-done = bf16[512,1024]{1,0:T(8,128)(2,1)} async-done(((bf16[2048,1024]{1,0:T(8,128)(2,1)}), bf16[512,1024]{1,0:T(8,128)(2,1)}) %reduce-scatter.3.cloned.1.call-update) | async-done | bytes 1048592 | tf_op jit(solution)/shard_map/reduce_scatter | solution.py:137
  338.7 2.6 add_convert_fusion.1
  341.4 0.9 constant_dynamic-slice_fusion.3
  343.5 32.4 %all-gather.19.cloned.1.call-done = bf16[2048,1024]{1,0:T(8,128)(2,1)} async-done(((bf16[512,1024]{1,0:T(8,128)(2,1)}), bf16[2048,1024]{1,0:T(8,128)(2,1)}) %all-gather.19.cloned.1.call-update) | async-done | bytes 4194320 | tf_op jit(solution)/shard_map/all_gather | solution.py:130
  376.0 9.7 %copy.91 = f32[2,2,512,1024]{3,1,2,0:T(2,128)} copy(bf16[2,2,512,1024]{3,2,1,0:T(8,128)(2,1)} %bitcast.108) | data formatting | bytes 12582912 | tf_op jit(solution)/shard_map/convert_element_type | solution.py:17
  385.7 11.1 %copy.116 = f32[128,8,2,1024]{3,1,2,0:T(8,128)} copy(f32[128,8,2,1024]{3,2,1,0:T(2,128)} %bitcast.105) | data formatting | bytes 16777216
  396.9 0.9 multiply_reduce_fusion
  397.8 53.0 %all-gather.13.cloned.1.call-done = bf16[2048,1024]{1,0:T(8,128)(2,1)} async-done(((bf16[256,1024]{1,0:T(8,128)(2,1)}), bf16[2048,1024]{1,0:T(8,128)(2,1)}) %all-gather.13.cloned.1.call-update) | async-done | bytes 4194320 | tf_op jit(solution)/shard_map/all_gather | solution.py:175
  450.8 75.2 %all-gather.15.cloned.1.call-done = bf16[1024,2048]{1,0:T(8,128)(2,1)} async-done(((bf16[1024,256]{1,0:T(8,128)(2,1)}), bf16[1024,2048]{1,0:T(8,128)(2,1)}) %all-gather.15.cloned.1.call-update) | async-done | bytes 4194320 | tf_op jit(solution)/shard_map/all_gather | solution.py:178
  526.0 15.6 %convolution_convert_fusion = bf16[1024,2048]{1,0:T(8,128)(2,1)} fusion(bf16[1024,2048]{1,0:T(8,128)(2,1)} %all-gather.15.cloned.1.call-done, bf16[2048,1024]{1,0:T(8,128)(2,1)} %all-gather.13.cloned.1.call-done, f32[1024,2048]{1,0:T(8,128)} %bitcast.116, f32[2048]{0:T(1024)S(1)} %copy-done.28, f32[1024]{0:T(1024)S(1)} %bitcast.129), kind=kOutput, calls=%fused_computation.48 | convolution fusion | flops 8601468928 | bytes 20983808 | tf_op jit(solution)/shard_map/dot_general | solution.py:179
  541.6 7.8 %reshape.238 = bf16[2,512,2,1024]{3,2,1,0:T(2,128)(2,1)} reshape(bf16[1024,2048]{1,0:T(8,128)(2,1)} %convolution_convert_fusion) | data formatting | bytes 8388608 | tf_op jit(solution)/shard_map/reshape | solution.py:135
  549.4 5.6 copy.92
  555.0 42.9 %reduce-scatter.5.cloned.1.call-done = bf16[512,1024]{1,0:T(8,128)(2,1)} async-done(((bf16[2048,1024]{1,0:T(8,128)(2,1)}), bf16[512,1024]{1,0:T(8,128)(2,1)}) %reduce-scatter.5.cloned.1.call-update) | async-done | bytes 1048592 | tf_op jit(solution)/shard_map/reduce_scatter | solution.py:137
  597.9 2.6 add_convert_fusion
  (155 shorter events, 8.2 us)
Async XLA Ops:
  6.5 1.2 copy-start
  6.5 3.5 copy-start.17
  6.5 39.6 %all-gather.17.cloned.1.call-start = ((), (), s32[]{:S(2)}) async-start(), calls=%async_computation.8 | async-start | bytes 5242880 | tf_op jit(solution)/shard_map/all_gather | solution.py:130
  7.3 165.5 %all-gather.9.cloned.1.call-start = ((), (), s32[]{:S(2)}) async-start(), calls=%async_computation.2 | async-start | bytes 9437184 | tf_op jit(solution)/shard_map/all_gather | solution.py:146
  10.0 261.3 %all-gather.11.cloned.1.call-start = ((), (), s32[]{:S(2)}) async-start(), calls=%async_computation.3 | async-start | bytes 4718592 | tf_op jit(solution)/shard_map/all_gather | solution.py:171
  10.9 327.8 %reduce-scatter.3.cloned.1.call-start = ((), (), s32[]{:S(2)}) async-start(), calls=%async_computation.4 | async-start | bytes 5242880 | tf_op jit(solution)/shard_map/reduce_scatter | solution.py:137
  55.9 11.5 %copy-start.2 = (bf16[2048,1024]{1,0:T(8,128)(2,1)S(1)}, bf16[2048,1024]{1,0:T(8,128)(2,1)}, u32[]{:S(2)}) copy-start(bf16[2048,1024]{1,0:T(8,128)(2,1)} %all-gather.17.cloned.1.call-done) | copy-start | bytes 12582916
  67.4 105.4 %copy-start.27 = (f32[2048]{0:T(1024)S(1)}, f32[2048]{0:T(1024)}, u32[]{:S(2)}) copy-start(f32[2048]{0:T(1024)} %param.13) | copy-start | bytes 24580
  187.0 4.6 copy-start.8
  201.3 1.9 copy-start.12
  201.3 2.0 copy-start.13
  201.3 2.1 copy-start.14
  209.3 8.1 %copy-start.15 = (bf16[1024,2,128]{2,0,1:T(8,128)(2,1)S(1)}, bf16[1024,2,128]{2,0,1:T(8,128)(2,1)}, u32[]{:S(2)}) copy-start(bf16[1024,2,128]{2,0,1:T(8,128)(2,1)} %get-tuple-element.269) | copy-start | bytes 1572868
  209.3 8.1 %copy-start.16 = (bf16[1024,2,128]{2,0,1:T(8,128)(2,1)S(1)}, bf16[1024,2,128]{2,0,1:T(8,128)(2,1)}, u32[]{:S(2)}) copy-start(bf16[1024,2,128]{2,0,1:T(8,128)(2,1)} %get-tuple-element.270) | copy-start | bytes 1572868
  213.9 4.6 copy-start.10
  214.0 4.6 copy-start.11
  218.7 2.6 copy-start.6
  218.7 3.9 copy-start.20
  218.7 3.9 copy-start.22
  218.8 3.9 copy-start.24
  226.2 2.2 copy-start.7
  226.2 2.2 copy-start.21
  226.2 2.2 copy-start.23
  226.2 2.2 copy-start.25
  228.4 2.6 copy-start.6
  228.4 3.9 copy-start.20
  228.4 3.9 copy-start.22
  228.5 3.9 copy-start.24
  235.9 2.2 copy-start.7
  235.9 2.2 copy-start.21
  235.9 2.2 copy-start.23
  235.9 2.2 copy-start.25
  238.2 2.6 copy-start.6
  238.2 3.9 copy-start.20
  238.2 3.9 copy-start.22
  238.2 3.9 copy-start.24
  245.6 2.2 copy-start.7
  245.6 2.2 copy-start.21
  245.6 2.2 copy-start.23
  245.6 2.2 copy-start.25
  247.8 2.6 copy-start.6
  247.9 3.9 copy-start.20
  247.9 3.9 copy-start.22
  247.9 3.9 copy-start.24
  255.3 2.2 copy-start.7
  255.3 2.2 copy-start.21
  255.3 2.2 copy-start.23
  255.3 2.2 copy-start.25
  261.9 3.0 copy-start.4
  268.2 3.1 copy-start.26
  295.8 43.0 %copy-start.9 = (bf16[512,1024]{1,0:T(8,128)(2,1)S(1)}, bf16[512,1024]{1,0:T(8,128)(2,1)}, u32[]{:S(2)}) copy-start(bf16[512,1024]{1,0:T(8,128)(2,1)} %param.12) | copy-start | bytes 3145732
  295.8 45.6 %copy-start.18 = (bf16[256,2048]{1,0:T(8,128)(2,1)S(1)}, bf16[256,2048]{1,0:T(8,128)(2,1)}, u32[]{:S(2)}) copy-start(bf16[256,2048]{1,0:T(8,128)(2,1)} %param.20) | copy-start | bytes 3145732
  295.8 46.6 %copy-start.19 = (bf16[2048,256]{1,0:T(8,128)(2,1)S(1)}, bf16[2048,256]{1,0:T(8,128)(2,1)}, u32[]{:S(2)}) copy-start(bf16[2048,256]{1,0:T(8,128)(2,1)} %param.21) | copy-start | bytes 3145732
  295.8 80.2 %all-gather.19.cloned.1.call-start = ((), (), s32[]{:S(2)}) async-start(), calls=%async_computation.9 | async-start | bytes 5242880 | tf_op jit(solution)/shard_map/all_gather | solution.py:130
  341.3 109.4 %all-gather.13.cloned.1.call-start = ((), (), s32[]{:S(2)}) async-start(), calls=%async_computation.5 | async-start | bytes 4718592 | tf_op jit(solution)/shard_map/all_gather | solution.py:175
  342.3 183.7 %all-gather.15.cloned.1.call-start = ((), (), s32[]{:S(2)}) async-start(), calls=%async_computation.6 | async-start | bytes 4718592 | tf_op jit(solution)/shard_map/all_gather | solution.py:178
  343.2 254.7 %reduce-scatter.5.cloned.1.call-start = ((), (), s32[]{:S(2)}) async-start(), calls=%async_computation.7 | async-start | bytes 5242880 | tf_op jit(solution)/shard_map/reduce_scatter | solution.py:137
  385.7 11.1 %copy-start.3 = (bf16[2048,1024]{1,0:T(8,128)(2,1)S(1)}, bf16[2048,1024]{1,0:T(8,128)(2,1)}, u32[]{:S(2)}) copy-start(bf16[2048,1024]{1,0:T(8,128)(2,1)} %all-gather.19.cloned.1.call-done) | copy-start | bytes 12582916
  396.9 129.2 %copy-start.28 = (f32[2048]{0:T(1024)S(1)}, f32[2048]{0:T(1024)}, u32[]{:S(2)}) copy-start(f32[2048]{0:T(1024)} %param.19) | copy-start | bytes 24580
  549.3 51.2 %copy-start.1 = (bf16[256,2048]{1,0:T(8,128)(2,1)S(1)}, bf16[256,2048]{1,0:T(8,128)(2,1)}, u32[]{:S(2)}) copy-start(bf16[256,2048]{1,0:T(8,128)(2,1)} %param.16) | copy-start | bytes 3145732
  555.0 42.9 %copy-start.5 = (bf16[512,1024]{1,0:T(8,128)(2,1)S(1)}, bf16[512,1024]{1,0:T(8,128)(2,1)}, u32[]{:S(2)}) copy-start(bf16[512,1024]{1,0:T(8,128)(2,1)} %add_convert_fusion.1) | copy-start | bytes 3145732
Sparse Core Ops, SparseCore 0:
  8.9 37.1 all-gather.16
  48.2 124.4 all-gather.8
  174.8 72.8 all-gather.10
  295.9 42.7 reduce-scatter.2
  341.5 34.4 all-gather.18
  377.9 72.7 all-gather.12
  452.8 73.1 all-gather.14
  555.1 42.7 reduce-scatter.4

commit v2 on v1

--- a/solution.py
+++ b/solution.py
@@ -1,6 +1,10 @@
+import functools
+
 import jax
 import jax.numpy as jnp
 from jax import lax
+from jax.experimental import pallas as pl
+from jax.experimental.pallas import tpu as pltpu
 from jax.sharding import PartitionSpec as P
 
 DK = 256
@@ -114,13 +118,118 @@
     return (middle.astype(jnp.float32) + channel).astype(jnp.bfloat16)
 
 
+def ring_place(spot, count):
+    turn = spot // (count // 2)
+    return (1 - turn) * 2 * spot + turn * (2 * (count - 1 - spot) + 1)
+
+
+def ring_kernel(count, axes, *refs):
+    kinds = len(axes)
+    sources, gathered = refs[:kinds], refs[kinds : 2 * kinds]
+    send_sem, recv_sem, own_sem = refs[2 * kinds :]
+    me = lax.axis_index("fs")
+    column, level = me % 2, me // 2
+    spot = (1 - column) * level + column * (count - 1 - level)
+    ahead = ring_place((spot + 1) % count, count)
+    behind = ring_place((spot + count - 1) % count, count)
+    barrier = pltpu.get_barrier_semaphore()
+    for other in (ahead, behind):
+        pl.semaphore_signal(
+            barrier, inc=1, device_id={"fs": other}, device_id_type=pl.DeviceIdType.MESH
+        )
+    pl.semaphore_wait(barrier, 2)
+    steps = count // 2
+
+    def slot(kind, origin):
+        rows, columns = sources[kind].shape
+        if axes[kind] == 0:
+            return gathered[kind].at[pl.ds(pl.multiple_of(origin * rows, rows), rows), :]
+        return gathered[kind].at[:, pl.ds(pl.multiple_of(origin * columns, columns), columns)]
+
+    def piece(kind, origin, part):
+        rows, columns = sources[kind].shape
+        size = rows // 2
+        if axes[kind] == 0:
+            start = pl.multiple_of(origin * rows + part * size, size)
+            return gathered[kind].at[pl.ds(start, size), :]
+        start = pl.multiple_of(origin * columns, columns)
+        return gathered[kind].at[pl.ds(part * size, size), pl.ds(start, columns)]
+
+    def used(way, step, part):
+        return step < steps - 1 or way == part
+
+    def copy(kind, way, step, part):
+        offset = count - step if way == 0 else step
+        origin = ring_place((spot + offset) % count, count)
+        target = piece(kind, origin, part)
+        size = sources[kind].shape[0] // 2
+        source = sources[kind].at[pl.ds(part * size, size), :] if step == 0 else target
+        return pltpu.make_async_remote_copy(
+            src_ref=source,
+            dst_ref=target,
+            send_sem=send_sem.at[kind, way, step, part],
+            recv_sem=recv_sem.at[kind, way, step, part],
+            device_id={"fs": ahead if way == 0 else behind},
+            device_id_type=pl.DeviceIdType.MESH,
+        )
+
+    def own(kind):
+        return pltpu.make_async_copy(sources[kind], slot(kind, me), own_sem.at[kind])
+
+    for kind in range(kinds):
+        own(kind).start()
+        for step in range(steps):
+            for part in range(2):
+                for way in range(2):
+                    if used(way, step, part):
+                        if step > 0:
+                            copy(kind, way, step - 1, part).wait_recv()
+                        copy(kind, way, step, part).start()
+    for kind in range(kinds):
+        own(kind).wait()
+        for step in range(steps):
+            for part in range(2):
+                for way in range(2):
+                    if used(way, step, part):
+                        copy(kind, way, step, part).wait_send()
+                        last = step == steps - 1 or not used(way, step + 1, part)
+                        if last:
+                            copy(kind, way, step, part).wait_recv()
+
+
+def ring_gather(count, axes, shards_in):
+    shapes = []
+    for axis, shard in zip(axes, shards_in):
+        shape = list(shard.shape)
+        shape[axis] *= count
+        shapes.append(jax.ShapeDtypeStruct(tuple(shape), shard.dtype))
+    kinds = len(axes)
+    sems = (kinds, 2, count // 2, 2)
+    return pl.pallas_call(
+        functools.partial(ring_kernel, count, axes),
+        out_shape=shapes,
+        in_specs=[pl.BlockSpec(memory_space=pltpu.VMEM)] * kinds,
+        out_specs=[pl.BlockSpec(memory_space=pl.ANY)] * kinds,
+        scratch_shapes=[
+            pltpu.SemaphoreType.DMA(sems),
+            pltpu.SemaphoreType.DMA(sems),
+            pltpu.SemaphoreType.DMA((kinds,)),
+        ],
+        compiler_params=pltpu.CompilerParams(collective_id=0, has_side_effects=True),
+        cost_estimate=pl.CostEstimate(
+            flops=40_000_000_000, bytes_accessed=60_000_000, transcendentals=0
+        ),
+        name="ring_gather",
+    )(*shards_in)
+
+
 def half_of(block, axis, index, count):
     size = block.shape[axis] // count
     return lax.dynamic_slice_in_dim(block, index * size, size, axis)
 
 
 def split_shards(
-    parts, tps, tokens, mix_gain, query_w, key_w, value_w, head_gain, out_w, chan_gain, up_w, down_w
+    parts, tps, count, tokens, mix_gain, query_w, key_w, value_w, head_gain, out_w, chan_gain, up_w, down_w
 ):
     rows, width = tokens.shape
     group = ("rep", "tp")
@@ -140,12 +249,14 @@
     mine = jnp.concatenate(
         [half_of(w, 1, rep, parts) for w in (query_w, key_w, value_w)], axis=1
     )
+    out_half = half_of(out_w, 0, rep, parts)
+    up_half = half_of(up_w, 1, rep, parts)
+    down_half = half_of(down_w, 0, rep, parts)
+    front_all, out_all, up_all, down_all = ring_gather(
+        count, (0, 1, 0, 1), (mine, out_half, up_half, down_half)
+    )
     normed = norm_rows(join(tokens), mix_gain)
-    raw = jnp.dot(
-        normed,
-        lax.all_gather(mine, "fs", axis=0, tiled=True),
-        preferred_element_type=jnp.float32,
-    )
+    raw = jnp.dot(normed, front_all, preferred_element_type=jnp.float32)
     qraw, kraw, vraw = jnp.split(raw, [local * DK, 2 * local * DK], axis=1)
     places = jnp.arange(rows, dtype=jnp.int32).astype(jnp.float32)
     places = jnp.tile(places, parts)
@@ -168,14 +279,11 @@
     gains = lax.dynamic_slice_in_dim(head_gain, first_head, local, 0)
     scale = lax.rsqrt(jnp.mean(retained * retained, axis=-1, keepdims=True) + HEAD_EPS)
     head_out = (retained * scale * gains).astype(jnp.bfloat16).reshape(parts * rows, local * DV)
-    out_all = lax.all_gather(half_of(out_w, 0, rep, parts), "fs", axis=1, tiled=True)
     mixed = scatter(jnp.dot(head_out, out_all, preferred_element_type=jnp.float32))
     middle = (tokens.astype(jnp.float32) + mixed).astype(jnp.bfloat16)
     chan_normed = norm_rows(join(middle), chan_gain)
-    up_all = lax.all_gather(half_of(up_w, 1, rep, parts), "fs", axis=0, tiled=True)
     upward = jnp.dot(chan_normed, up_all, preferred_element_type=jnp.float32)
     hidden = jnp.square(jax.nn.relu(upward)).astype(jnp.bfloat16)
-    down_all = lax.all_gather(half_of(down_w, 0, rep, parts), "fs", axis=1, tiled=True)
     channel = scatter(jnp.dot(hidden, down_all, preferred_element_type=jnp.float32))
     return (middle.astype(jnp.float32) + channel).astype(jnp.bfloat16)
 
@@ -193,11 +301,11 @@
         P("fs", "tp"),
         P("tp", "fs"),
     )
-    parts, tps = mesh.shape["rep"], mesh.shape["tp"]
+    parts, tps, count = mesh.shape["rep"], mesh.shape["tp"], mesh.shape["fs"]
 
     def body(*blocks):
-        if blocks[2].shape[1] // DK % parts == 0:
-            return split_shards(parts, tps, *blocks)
+        if blocks[2].shape[1] // DK % parts == 0 and count % 2 == 0:
+            return split_shards(parts, tps, count, *blocks)
         return shards(*blocks)
 
     return jax.shard_map(

time: 617 us -> 555 us (0.90)
  waiting for transfers between devices: 382 us -> 124 us
  Pallas kernels: 0 us -> 208 us
    all_gather x4 -> x0, waiting for transfers between devices: 233 us -> none  [the longest x1 104 us: split_shards(): lax.all_gather(mine, 'fs', axis=0, tiled=True)]
    pallas_call x0 -> x1, Pallas kernels: none -> 208 us  [ring_gather(): pl.pallas_call(functools.partial(ring_kernel, count, axes), out_shape=sha...]
    all_gather x2, waiting for transfers between devices: 62.4 us -> 34.3 us  [join(): whole = lax.all_gather(block, group, axis=0, tiled=False)]
    unnamed x52 -> x44, local copies, waits for them, and re-layouts: 32.5 us -> 26.8 us
  transfers between devices with their start and end apart: 8 -> 4, of which waited for: 7 -> 3; matrix products, arithmetic and copies ran while one was open for 25% -> 2% of each run, Pallas kernels for 0% -> 38%
where the time goes in v2:
time: 555 us; the launch traced here: 545 us
  Pallas kernels  208 us (37%)
  waiting for transfers between devices  124 us (22%)
  local copies, waits for them, and re-layouts  116 us (21%)
  matrix products  60 us (11%)
  other arithmetic  22.7 us (4%)
  between operations  13.9 us (3%)
    pallas_call x1, Pallas kernels, ring_gather(): pl.pallas_call(functools.partial(ring_kernel, count, axes), out_shape=sha...  208 us
    reduce_scatter x2, waiting for transfers between devices, scatter(): lax.psum_scatter(pieces, group, scatter_dimension=0, tiled=True)  88.5 us
    all_gather x2, waiting for transfers between devices, join(): whole = lax.all_gather(block, group, axis=0, tiled=False)  34.3 us
    unnamed x44, local copies, waits for them, and re-layouts  26.8 us
    convert_element_type x2, local copies, waits for them, and re-layouts, norm_rows(): values = rows.astype(jnp.float32)  19.5 us
    reshape x2, local copies, waits for them, and re-layouts, scatter(): terms.astype(jnp.bfloat16).reshape(parts, rows, tps, width)  15.6 us
    dot_general x1, matrix products, split_shards(): jnp.dot(hidden, down_all, preferred_element_type=jnp.float32)  15.6 us
    dot_general x1, matrix products, split_shards(): raw = jnp.dot(normed, front_all, preferred_element_type=jnp.float32)  13.9 us
  transfers between devices with their start and end apart: 4, of which 3 were waited for; matrix products, arithmetic and copies ran while one was open for 2% of the time, Pallas kernels for 38%

profile of v2, /device:TPU:0, one launch (start us, length us, event | category | flops | bytes accessed | tf_op | source)
XLA Modules:
  0.0 545.1 jit_solution(14572677586049583820)
XLA Ops:
  6.5 0.7 all-gather.5.cloned.1.call-update
  8.7 1.1 constant_dynamic-slice_fusion.6
  9.8 2.1 constant_dynamic-slice_fusion.3
  11.9 2.1 constant_dynamic-slice_fusion.2
  14.0 1.1 pad_maximum_fusion.refs_0_
  15.1 3.1 multiply_cosine_fusion
  18.2 207.8 %ring_gather.1 = (bf16[2048,2048]{1,0:T(8,128)(2,1)}, bf16[1024,2048]{1,0:T(8,128)(2,1)}, bf16[2048,1024]{1,0:T(8,128)(2,1)}, bf16[1024,2048]{1,0:T(8,128)(2,1)}) custom-call(bf16[256,2048]{1,0:T(8,128)(2,1)} %pad_maximum_fusion.refs_0_, bf16[1024,256]{1,0:T(8,128)(2,1)} %get-tuple-element.290.refs_1_, bf16[256,1024]{1,0:T(8,128)(2,1)} %get-tuple-element.291.refs_2_, ...), custom_call_target="tpu_custom_call" | custom-call | flops 40000000000 | bytes 60000000 | tf_op jit(solution)/shard_map/ring_gather/pallas_call | solution.py:208
  226.0 9.8 %copy.76 = f32[2,2,512,1024]{3,1,2,0:T(2,128)} copy(bf16[2,2,512,1024]{3,2,1,0:T(8,128)(2,1)} %bitcast.107) | data formatting | bytes 12582912 | tf_op jit(solution)/shard_map/convert_element_type | solution.py:21
  235.8 10.9 %copy.110 = f32[128,8,2,1024]{3,1,2,0:T(8,128)} copy(f32[128,8,2,1024]{3,2,1,0:T(2,128)} %bitcast.104) | data formatting | bytes 16777216
  246.7 0.9 multiply_reduce_fusion.1
  247.7 13.9 %fusion.24 = f32[1024,2048]{1,0:T(8,128)S(1)} fusion(bf16[2048,2048]{1,0:T(8,128)(2,1)} %get-tuple-element.61, f32[1024,2048]{1,0:T(8,128)} %bitcast.117, f32[2048]{0:T(1024)S(1)} %copy-done.22, f32[1024]{0:T(1024)S(1)} %bitcast.130), kind=kOutput, calls=%fused_computation.38 | convolution fusion | flops 8596226048 | bytes 25178112 | tf_op jit(solution)/shard_map/dot_general | solution.py:259
  261.6 2.5 fusion.36
  264.1 1.7 split.17
  265.8 3.6 reshape.232
  269.4 2.6 fusion.37
  272.1 3.5 reshape.229
  275.6 3.1 fusion.38
  278.7 4.5 convert_element_type.142
  283.2 3.4 copy.80
  287.2 1.1 pad_maximum_fusion.1
  288.4 39.0 %while.15 = (s32[]{:T(128)}, f32[2,2,256,512]{3,2,1,0:T(8,128)S(1)}, f32[4,2,2,128,512]{4,3,0,2,1:T(8,128)}, bf16[4,2,2,128,256]{4,3,0,1,2:T(8,128)(2,1)S(1)}, b...) while((s32[]{:T(128)}, ...), condition=%wide.region_3.4_spmd.clone.clone.clone, body=%wide.region_2.3_spmd.clone.clone.clone.sunk | while | flops 372441600 | bytes 21330904 | solution.py:67
  288.5 1.9 constant_dynamic-slice_fusion.9
  290.4 0.7 multiply_exponential_fusion.6
  291.1 1.3 fusion.49
  292.5 0.9 exponential_select_fusion.2
  293.4 2.6 fusion.50
  296.0 2.2 multiply_add_fusion.3
  298.3 1.9 constant_dynamic-slice_fusion.9
  300.2 0.7 multiply_exponential_fusion.6
  300.8 1.3 fusion.49
  302.2 0.9 exponential_select_fusion.2
  303.1 2.5 fusion.50
  305.7 2.2 multiply_add_fusion.3
  308.0 1.9 constant_dynamic-slice_fusion.9
  310.6 1.3 fusion.49
  311.9 0.9 exponential_select_fusion.2
  312.9 2.6 fusion.50
  315.5 2.2 multiply_add_fusion.3
  317.7 1.9 constant_dynamic-slice_fusion.9
  320.3 1.3 fusion.49
  321.7 0.9 exponential_select_fusion.2
  322.6 2.6 fusion.50
  325.2 2.2 multiply_add_fusion.3
  327.5 2.5 multiply_reduce_fusion.2
  330.2 1.6 mul.349
  331.9 1.0 copy.114
  332.9 1.1 copy-done.4
  334.0 3.2 copy.88
  337.3 1.0 copy.113
  338.4 1.1 copy-done.24
  339.5 6.2 %convolution_convert_fusion.1 = bf16[1024,2048]{1,0:T(8,128)(2,1)} fusion(bf16[1024,2048]{1,0:T(8,128)(2,1)S(1)} %copy-done.24, f32[1024,1024]{1,0:T(8,128)S(1)} %bitcast.121, f32[1024,1024]{1,0:T(8,128)S(1)} %bitcast.120, f32[1024]{0:T(1024)S(1)} %bitcast.128), kind=kOutput, calls=%fused_computation.49 | convolution fusion | flops 4300210176 | bytes 16781312 | tf_op jit(solution)/shard_map/dot_general | solution.py:282
  345.7 7.8 %reshape.236 = bf16[2,512,2,1024]{3,2,1,0:T(2,128)(2,1)} reshape(bf16[1024,2048]{1,0:T(8,128)(2,1)} %convolution_convert_fusion.1) | data formatting | bytes 8388608 | tf_op jit(solution)/shard_map/reshape | solution.py:244
  353.5 5.5 %copy.90 = bf16[2,2,512,1024]{3,2,1,0:T(8,128)(2,1)} copy(bf16[2,2,512,1024]{3,1,2,0:T(2,128)(2,1)} %bitcast.114) | data formatting | bytes 8388608 | tf_op jit(solution)/shard_map/transpose | solution.py:244
  359.1 43.8 %reduce-scatter.3.cloned.1.call-done = bf16[512,1024]{1,0:T(8,128)(2,1)} async-done(((bf16[2048,1024]{1,0:T(8,128)(2,1)}), bf16[512,1024]{1,0:T(8,128)(2,1)}) %reduce-scatter.3.cloned.1.call-update) | async-done | bytes 1048592 | tf_op jit(solution)/shard_map/reduce_scatter | solution.py:246
  402.9 2.6 add_convert_fusion.1
  405.8 34.3 %all-gather.7.cloned.1.call-done = bf16[2048,1024]{1,0:T(8,128)(2,1)} async-done(((bf16[512,1024]{1,0:T(8,128)(2,1)}), bf16[2048,1024]{1,0:T(8,128)(2,1)}) %all-gather.7.cloned.1.call-update) | async-done | bytes 4194320 | tf_op jit(solution)/shard_map/all_gather | solution.py:239
  440.1 9.7 %copy.91 = f32[2,2,512,1024]{3,1,2,0:T(2,128)} copy(bf16[2,2,512,1024]{3,2,1,0:T(8,128)(2,1)} %bitcast.108) | data formatting | bytes 12582912 | tf_op jit(solution)/shard_map/convert_element_type | solution.py:21
  449.9 10.9 %copy.116 = f32[128,8,2,1024]{3,1,2,0:T(8,128)} copy(f32[128,8,2,1024]{3,2,1,0:T(2,128)} %bitcast.105) | data formatting | bytes 16777216
  460.8 0.9 multiply_reduce_fusion
  461.8 15.6 %convolution_convert_fusion = bf16[1024,2048]{1,0:T(8,128)(2,1)} fusion(bf16[1024,2048]{1,0:T(8,128)(2,1)} %get-tuple-element.65, bf16[2048,1024]{1,0:T(8,128)(2,1)} %get-tuple-element.64, f32[1024,2048]{1,0:T(8,128)} %bitcast.116, f32[2048]{0:T(1024)S(1)} %copy-done.23, f32[1024]{0:T(1024)S(1)} %bitcast.129), kind=kOutput, calls=%fused_computation.48 | convolution fusion | flops 8601468928 | bytes 20983808 | tf_op jit(solution)/shard_map/dot_general | solution.py:287
  477.3 7.8 %reshape.238 = bf16[2,512,2,1024]{3,2,1,0:T(2,128)(2,1)} reshape(bf16[1024,2048]{1,0:T(8,128)(2,1)} %convolution_convert_fusion) | data formatting | bytes 8388608 | tf_op jit(solution)/shard_map/reshape | solution.py:244
  485.1 5.5 %copy.92 = bf16[2,2,512,1024]{3,2,1,0:T(8,128)(2,1)} copy(bf16[2,2,512,1024]{3,1,2,0:T(2,128)(2,1)} %bitcast.115) | data formatting | bytes 8388608 | tf_op jit(solution)/shard_map/transpose | solution.py:244
  490.7 44.7 %reduce-scatter.5.cloned.1.call-done = bf16[512,1024]{1,0:T(8,128)(2,1)} async-done(((bf16[2048,1024]{1,0:T(8,128)(2,1)}), bf16[512,1024]{1,0:T(8,128)(2,1)}) %reduce-scatter.5.cloned.1.call-update) | async-done | bytes 1048592 | tf_op jit(solution)/shard_map/reduce_scatter | solution.py:246
  535.4 2.6 add_convert_fusion
  (134 shorter events, 4.4 us)
Async XLA Ops:
  6.5 0.8 copy-start
  6.5 5.4 copy-start.14
  6.5 219.5 %all-gather.5.cloned.1.call-start = ((), (), s32[]{:S(2)}) async-start(), calls=%async_computation.4 | async-start | bytes 5242880 | tf_op jit(solution)/shard_map/all_gather | solution.py:239
  7.3 395.6 %reduce-scatter.3.cloned.1.call-start = ((), (), s32[]{:S(2)}) async-start(), calls=%async_computation.2 | async-start | bytes 5242880 | tf_op jit(solution)/shard_map/reduce_scatter | solution.py:246
  235.8 10.9 %copy-start.2 = (bf16[2048,1024]{1,0:T(8,128)(2,1)S(1)}, bf16[2048,1024]{1,0:T(8,128)(2,1)}, u32[]{:S(2)}) copy-start(bf16[2048,1024]{1,0:T(8,128)(2,1)} %all-gather.5.cloned.1.call-done) | copy-start | bytes 12582916
  246.7 1.0 copy-start.22
  283.2 3.5 copy-start.9
  283.2 3.5 copy-start.10
  283.2 3.5 copy-start.11
  283.2 3.5 copy-start.12
  283.2 3.5 copy-start.13
  288.5 2.6 copy-start.6
  288.5 4.0 copy-start.15
  288.5 4.0 copy-start.17
  288.5 4.0 copy-start.19
  296.0 2.2 copy-start.7
  296.0 2.2 copy-start.16
  296.0 2.2 copy-start.18
  296.0 2.2 copy-start.20
  298.2 2.6 copy-start.6
  298.2 4.0 copy-start.15
  298.2 4.0 copy-start.17
  298.2 4.0 copy-start.19
  305.7 2.2 copy-start.7
  305.7 2.2 copy-start.16
  305.7 2.2 copy-start.18
  305.7 2.2 copy-start.20
  307.9 2.6 copy-start.6
  308.0 4.0 copy-start.15
  308.0 4.0 copy-start.17
  308.0 4.0 copy-start.19
  315.4 2.2 copy-start.7
  315.4 2.2 copy-start.16
  315.4 2.2 copy-start.18
  315.4 2.2 copy-start.20
  317.7 2.6 copy-start.6
  317.7 4.0 copy-start.15
  317.7 4.0 copy-start.17
  317.7 4.0 copy-start.19
  325.2 2.2 copy-start.7
  325.2 2.2 copy-start.16
  325.2 2.2 copy-start.18
  325.2 2.2 copy-start.20
  331.9 2.2 copy-start.4
  337.3 1.1 copy-start.21
  337.3 2.2 copy-start.24
  359.0 43.9 %copy-start.8 = (bf16[512,1024]{1,0:T(8,128)(2,1)S(1)}, bf16[512,1024]{1,0:T(8,128)(2,1)}, u32[]{:S(2)}) copy-start(bf16[512,1024]{1,0:T(8,128)(2,1)} %param.12) | copy-start | bytes 3145732
  359.0 81.1 %all-gather.7.cloned.1.call-start = ((), (), s32[]{:S(2)}) async-start(), calls=%async_computation.5 | async-start | bytes 5242880 | tf_op jit(solution)/shard_map/all_gather | solution.py:239
  405.5 129.9 %reduce-scatter.5.cloned.1.call-start = ((), (), s32[]{:S(2)}) async-start(), calls=%async_computation.3 | async-start | bytes 5242880 | tf_op jit(solution)/shard_map/reduce_scatter | solution.py:246
  449.8 11.0 %copy-start.3 = (bf16[2048,1024]{1,0:T(8,128)(2,1)S(1)}, bf16[2048,1024]{1,0:T(8,128)(2,1)}, u32[]{:S(2)}) copy-start(bf16[2048,1024]{1,0:T(8,128)(2,1)} %all-gather.7.cloned.1.call-done) | copy-start | bytes 12582916
  460.8 1.0 copy-start.23
  485.1 52.9 %copy-start.1 = (f32[8,512]{1,0:T(8,128)S(1)}, f32[8,512]{1,0:T(8,128)}, u32[]{:S(2)}) copy-start(f32[8,512]{1,0:T(8,128)} %param.17) | copy-start | bytes 49156
  490.7 44.8 %copy-start.5 = (bf16[512,1024]{1,0:T(8,128)(2,1)S(1)}, bf16[512,1024]{1,0:T(8,128)(2,1)}, u32[]{:S(2)}) copy-start(bf16[512,1024]{1,0:T(8,128)(2,1)} %add_convert_fusion.1) | copy-start | bytes 3145732
Sparse Core Ops, SparseCore 0:
  8.9 37.1 all-gather.4
  359.1 43.6 reduce-scatter.2
  405.6 34.4 all-gather.6
  490.8 44.5 reduce-scatter.4
